TPU v7x, 128 devices: a whole 4x4x4 slice. The times are simulated.
128 devices in a mesh: sp: 64 (over z, y, x), tp: 2 (over core).
Axes of the slice: x: 4, y: 4, z: 4, core: 2. Of those that a mesh axis runs over, the one named last changes fastest.
Arguments:
- stream: bfloat16 [16384, 2048], P(('sp', 'tp')), may hold values from -3 to 3
- query_narrow: bfloat16 [16384, 1024], P('sp', 'tp'), may hold values from -6 to 6
- key_narrow: bfloat16 [16384, 128], P('sp', 'tp'), may hold values from -6 to 6
- value_narrow: bfloat16 [16384, 128], P('sp', 'tp'), may hold values from -6 to 6
- query_broad: bfloat16 [16384, 1024], P('sp', 'tp'), may hold values from -6 to 6
- key_broad: bfloat16 [16384, 256], P('sp', 'tp'), may hold values from -6 to 6
- value_broad: bfloat16 [16384, 256], P('sp', 'tp'), may hold values from -6 to 6
- narrow_query_gain: float32 [64], replicated, may hold values from 1.5 to 9
- narrow_key_gain: float32 [64], replicated, may hold values from 1.5 to 9
- broad_query_gain: float32 [128], replicated, may hold values from 1.5 to 9
- broad_key_gain: float32 [128], replicated, may hold values from 1.5 to 9
- out_weight: bfloat16 [2048, 2048], replicated, may hold values from -0.125 to 0.125
- norm_gain: float32 [2048], replicated, may hold values from 0.1 to 1.9
- gate_weight: bfloat16 [64, 2048, 1024], P('sp', None, 'tp'), may hold values from -0.125 to 0.125
- up_weight: bfloat16 [64, 2048, 1024], P('sp', None, 'tp'), may hold values from -0.125 to 0.125
- down_weight: bfloat16 [64, 1024, 2048], P('sp', 'tp'), may hold values from -0.1875 to 0.1875
- route_ids: int32 [16384, 2], P(('sp', 'tp')), may hold values from 0 to 63, all different within a row; in each aligned block of 128 rows (0 to 127, 128 to 255, ...) at most 8 rows name the same one
- route_weights: float32 [16384, 2], P(('sp', 'tp')), may hold values from 0.1 to 1
Outputs:
- result: bfloat16 [16384, 2048], P(('sp', 'tp'))
Inputs may be any that keep to these rules, and one draw needn't show every extreme that they name: `route_ids`: in each aligned block of 128 rows no expert is named by more than 8 rows, a bound that some block reaches.
All inputs are finite; a program needn't handle non-finite values.
Results may differ from a plain program's by a relative error of at most 0.015.
The roundings to bfloat16 on the way count: a program that leaves them out, or rounds other values in their place, can miss the bound.
Values may be sent and summed in bfloat16 or wider, within the bound.
A program may use at most 128 MiB of HBM per device.

v0:
```python
import math
import jax
import jax.numpy as jnp
from jax import lax
from jax.sharding import PartitionSpec as P

HA = 16
DA = 64
DB = 128
GRID_W = 128
eps = 1e-06
theta = 10000.0


def cut_along(value, dim, size):
    before, after = (value.shape[:dim], value.shape[dim + 1 :])
    return jnp.moveaxis(value.reshape(*before, size, -1, *after), dim, 0)


def summed_on_arrival(value, axis, dim):
    size = lax.axis_size(axis)
    blocks = lax.all_to_all(cut_along(value, dim, size), axis, 0, 0, tiled=True)
    return jnp.sum(blocks.astype(jnp.float32), axis=0)


def joined_along(blocks, dim):
    shape = list(blocks.shape[1:])
    shape[dim] *= blocks.shape[0]
    return jnp.moveaxis(blocks, 0, dim).reshape(shape)


def copy_for_each(value, axis):
    size = lax.axis_size(axis)
    return lax.all_to_all(
        jnp.broadcast_to(value[None], (size, *value.shape)), axis, 0, 0, tiled=True
    )


def gather_directly(value, axis, dim):
    return joined_along(copy_for_each(value, axis), dim)


def rotate_grid(normed, positions):
    count, heads, dim = normed.shape
    freqs = dim // 4
    inverse = theta ** (-jnp.arange(freqs, dtype=jnp.float32) / freqs)
    rows = (positions // GRID_W).astype(jnp.float32)
    cols = (positions % GRID_W).astype(jnp.float32)
    angles = jnp.stack([rows[:, None] * inverse, cols[:, None] * inverse], axis=1)
    cosine = jnp.cos(angles)[:, None]
    sine = jnp.sin(angles)[:, None]
    split = normed.reshape(count, heads, 2, 2, freqs)
    first = split[..., 0, :]
    second = split[..., 1, :]
    turned = jnp.stack([first * cosine - second * sine, second * cosine + first * sine], axis=-2)
    return turned.reshape(count, heads, dim)


def prepare(raw, gain, dim, positions):
    count = raw.shape[0]
    values = raw.astype(jnp.float32).reshape(count, -1, dim)
    scaled = values * lax.rsqrt(jnp.mean(values * values, axis=-1, keepdims=True) + eps) * gain
    return rotate_grid(scaled, positions).reshape(count, -1).astype(jnp.bfloat16)


def arrange(queries, kv_width, dim):
    rows = queries.shape[0]
    heads_kv = kv_width // dim
    shaped = queries.reshape(rows, heads_kv, -1, dim)
    groups = shaped.shape[2]
    start = (
        jnp.full((heads_kv, groups, rows), -1e30, jnp.float32),
        jnp.zeros((heads_kv, groups, rows), jnp.float32),
        jnp.zeros((heads_kv, groups, rows, dim), jnp.float32),
    )
    return (shaped, start)


def attend_block(state, queries, keys, values):
    peak, total, summed = state
    dim = queries.shape[-1]
    scores = jnp.einsum(
        "qhgd,khd->hgqk", queries, keys, preferred_element_type=jnp.float32
    ) * dim ** (-0.5)
    fresh = jnp.maximum(peak, jnp.max(scores, axis=-1))
    weights = jnp.exp(scores - fresh[..., None])
    shrink = jnp.exp(peak - fresh)
    total = total * shrink + jnp.sum(weights, axis=-1)
    summed = summed * shrink[..., None] + jnp.einsum(
        "hgqk,khd->hgqd", weights.astype(jnp.bfloat16), values, preferred_element_type=jnp.float32
    )
    return (fresh, total, summed)


def sweep(state, keys, values, queries):
    rows = keys.shape[0]
    size = math.gcd(rows, 2048)
    count = rows // size

    def step(carry, block):
        return (attend_block(carry, queries, block[0], block[1]), None)

    blocks = (
        keys.reshape(count, size, keys.shape[1], keys.shape[2]),
        values.reshape(count, size, values.shape[1], values.shape[2]),
    )
    state, _ = lax.scan(step, state, blocks)
    return state


def make_fold(shaped_n, shaped_b, state, pieces):
    keys_n, values_n, keys_b, values_b = pieces
    rows = keys_n.shape[0]
    first = sweep(state[0], keys_n.reshape(rows, -1, DA), values_n.reshape(rows, -1, DA), shaped_n)
    second = sweep(state[1], keys_b.reshape(rows, -1, DB), values_b.reshape(rows, -1, DB), shaped_b)
    return (first, second)


def finish(state):
    peak, total, summed = state
    heads_out = summed / total[..., None]
    rows = heads_out.shape[2]
    return jnp.transpose(heads_out, (2, 0, 1, 3)).reshape(rows, -1).astype(jnp.bfloat16)


def local(
    stream,
    query_narrow,
    key_narrow,
    value_narrow,
    query_broad,
    key_broad,
    value_broad,
    narrow_query_gain,
    narrow_key_gain,
    broad_query_gain,
    broad_key_gain,
    out_weight,
    norm_gain,
    gate_weight,
    up_weight,
    down_weight,
    route_ids,
    route_weights,
):
    count = query_narrow.shape[0]
    positions = lax.axis_index("sp") * count + jnp.arange(count, dtype=jnp.int32)
    queries_n = prepare(query_narrow, narrow_query_gain, DA, positions)
    keys_n = prepare(key_narrow, narrow_key_gain, DA, positions)
    queries_b = prepare(query_broad, broad_query_gain, DB, positions)
    keys_b = prepare(key_broad, broad_key_gain, DB, positions)
    shaped_n, start_n = arrange(queries_n, keys_n.shape[1], DA)
    shaped_b, start_b = arrange(queries_b, keys_b.shape[1], DB)
    state = make_fold(
        shaped_n,
        shaped_b,
        (start_n, start_b),
        (
            lax.all_gather(keys_n, "sp", axis=0, tiled=True),
            lax.all_gather(value_narrow, "sp", axis=0, tiled=True),
            lax.all_gather(keys_b, "sp", axis=0, tiled=True),
            lax.all_gather(value_broad, "sp", axis=0, tiled=True),
        ),
    )
    heads_n = finish(state[0])
    heads_b = finish(state[1])
    width = heads_n.shape[1]
    place = lax.axis_index("tp")
    local_weight = jnp.concatenate(
        [
            lax.dynamic_slice_in_dim(out_weight, place * width, width, 0),
            lax.dynamic_slice_in_dim(out_weight, HA * DA + place * width, width, 0),
        ],
        axis=0,
    )
    local_heads = jnp.concatenate([heads_n, heads_b], axis=1)
    picked = local_heads
    mixed = summed_on_arrival(
        jnp.dot(picked, local_weight, preferred_element_type=jnp.float32).astype(jnp.bfloat16),
        "tp",
        0,
    )
    wide = (stream.astype(jnp.float32) + mixed).astype(jnp.bfloat16).astype(jnp.float32)
    normed = (
        wide * lax.rsqrt(jnp.mean(wide * wide, axis=-1, keepdims=True) + eps) * norm_gain
    ).astype(jnp.bfloat16)
    tokens_here, topk = route_ids.shape
    width_model = normed.shape[1]
    experts = lax.axis_size("sp")
    capacity = (2 * tokens_here * topk + experts - 1) // experts
    flat = route_ids.reshape(-1)
    hits = (flat[:, None] == jnp.arange(experts, dtype=jnp.int32)[None, :]).astype(jnp.int32)
    ranks = jnp.sum((jnp.cumsum(hits, axis=0) - 1) * hits, axis=1)
    slots = flat * capacity + ranks
    table = (jnp.arange(experts * capacity, dtype=jnp.int32)[:, None] == slots[None, :]).astype(
        jnp.bfloat16
    )
    table = jnp.sum(table.reshape(experts * capacity, tokens_here, topk), axis=2)
    sent = jnp.dot(table, normed, preferred_element_type=jnp.float32).astype(jnp.bfloat16)
    sent = sent.reshape(experts, capacity, width_model)
    piece = gather_directly(
        lax.all_to_all(sent, "sp", split_axis=0, concat_axis=0, tiled=True), "tp", 0
    )
    rows = piece.reshape(-1, piece.shape[-1])
    gate = jnp.dot(rows, gate_weight[0], preferred_element_type=jnp.float32)
    upper = jnp.dot(rows, up_weight[0], preferred_element_type=jnp.float32)
    hidden = (jax.nn.silu(gate) * upper).astype(jnp.bfloat16)
    partial_out = jnp.dot(hidden, down_weight[0], preferred_element_type=jnp.float32).astype(
        jnp.bfloat16
    )
    terms = lax.optimization_barrier(partial_out).astype(jnp.float32).reshape(piece.shape)
    summed = summed_on_arrival(terms.astype(jnp.bfloat16), "tp", 0).astype(jnp.bfloat16)
    back = lax.all_to_all(summed, "sp", split_axis=0, concat_axis=0, tiled=True)
    picked = jnp.take(back.reshape(experts * capacity, width_model), slots, axis=0)
    picked = picked.astype(jnp.float32).reshape(tokens_here, topk, width_model)
    routed = jnp.sum(picked * route_weights[..., None], axis=1)
    return (wide + routed).astype(jnp.bfloat16)


def solution(mesh):
    return jax.shard_map(
        local,
        mesh=mesh,
        in_specs=(
            P(("sp", "tp"), None),
            P("sp", "tp"),
            P("sp", "tp"),
            P("sp", "tp"),
            P("sp", "tp"),
            P("sp", "tp"),
            P("sp", "tp"),
            P(),
            P(),
            P(),
            P(),
            P(),
            P(),
            P("sp", None, "tp"),
            P("sp", None, "tp"),
            P("sp", "tp", None),
            P(("sp", "tp"), None),
            P(("sp", "tp"), None),
        ),
        out_specs=P(("sp", "tp"), None),
        check_vma=False,
    )
```

profile of v0, /device:TPU:0, one launch (start us, length us, event | category | flops | bytes accessed | tf_op | source)
XLA Modules:
  0.0 630.0 jit_solution(12985772197260481180)
XLA Ops:
  25.9 53.0 %all-gather.5.cloned.1.call-done = bf16[16384,64]{0,1:T(8,128)(2,1)} async-done(((bf16[256,64]{0,1:T(8,128)(2,1)}), bf16[16384,64]{0,1:T(8,128)(2,1)}) %all-gather.5.cloned.1.call-update) | async-done | bytes 2097168 | tf_op jit(solution)/shard_map/all_gather | solution.py:159
  84.2 63.0 %all-gather.7.cloned.1.call-done = bf16[16384,64]{0,1:T(8,128)(2,1)} async-done(((bf16[256,64]{0,1:T(8,128)(2,1)}), bf16[16384,64]{0,1:T(8,128)(2,1)}) %all-gather.7.cloned.1.call-update) | async-done | bytes 2097168 | tf_op jit(solution)/shard_map/all_gather | solution.py:160
  152.5 219.9 %while.30 = (s32[]{:T(128)}, f32[1,8,256]{2,1,0:T(8,128)S(1)}, f32[1,8,256]{2,1,0:T(8,128)S(1)}, f32[1,8,256,64]{2,3,1,0:T(8,128)}, bf16[8,2048,1,64]{1,3,2,0:T(...) while((s32[]{:T(128)}, f32[1,8,256]{2,1,0:T(8,128)S(1)}, ...), condition=%wide.region_5.6_spmd.clone, body=%wide.region_2.5_spmd.clone.sunk | while | flops 1107701760 | bytes 52298852 | solution.py:107
  152.8 9.0 %bitcast_reduce_fusion.6 = (f32[8,256]{1,0:T(8,128)S(1)}, f32[2048,256,8]{1,0,2:T(8,128)}) fusion(bf16[256,1,8,64]{0,3,2,1:T(8,128)(2,1)S(1)} %get-tuple-element.395, bf16[8,2048,1,64]{1,3,2,0:T(8,128)(2,1)} %get-tuple-element.394, s32[]{:T(128)} %get-tuple-element.381), kind=kOutput, calls=%fused_computation.2.clone.1 | convolution fusion | flops 545257472 | bytes 17310208 | tf_op jit(solution)/shard_map/while/body/eval_jaxpr/qhgd,khd->hgqk/dot_general | solution.py:82
  161.8 9.6 %fusion.116 = f32[1,8,256,64]{2,3,1,0:T(8,128)} fusion(f32[2048,256,8]{1,0,2:T(8,128)} %get-tuple-element.332, f32[8,256]{1,0:T(8,128)S(1)} %bitcast.237, f32[1,8,256,64]{2,3,1,0:T(8,128)} %get-tuple-element.384, bf16[8,2048,1,64]{1,3,2,0:T(8,128)(2,1)} %get-tuple-element.396, s32[]{:T(128)} %get-tuple-element.381, ...), kind=kOutput, calls=%fused_computation.9.clone.1 | convolution fusion | flops 549847040 | bytes 18104832 | tf_op jit(solution)/shard_map/while/body/eval_jaxpr/hgqk,khd->hgqd/dot_general | solution.py:89
  171.5 8.6 %fusion.115 = f32[8,256]{1,0:T(8,128)S(1)} fusion(f32[2048,256,8]{1,0,2:T(8,128)} %get-tuple-element.332, f32[8,256]{1,0:T(8,128)S(1)} %bitcast.238), kind=kLoop, calls=%fused_computation.5.clone.1 | loop fusion | flops 12580864 | bytes 16793600 | tf_op jit(solution)/shard_map/while/body/eval_jaxpr/reduce_sum | solution.py:88
  180.1 9.0 %bitcast_reduce_fusion.6 = (f32[8,256]{1,0:T(8,128)S(1)}, f32[2048,256,8]{1,0,2:T(8,128)}) fusion(bf16[256,1,8,64]{0,3,2,1:T(8,128)(2,1)S(1)} %get-tuple-element.395, bf16[8,2048,1,64]{1,3,2,0:T(8,128)(2,1)} %get-tuple-element.394, s32[]{:T(128)} %get-tuple-element.381), kind=kOutput, calls=%fused_computation.2.clone.1 | convolution fusion | flops 545257472 | bytes 17310208 | tf_op jit(solution)/shard_map/while/body/eval_jaxpr/qhgd,khd->hgqk/dot_general | solution.py:82
  189.1 9.7 %fusion.116 = f32[1,8,256,64]{2,3,1,0:T(8,128)} fusion(f32[2048,256,8]{1,0,2:T(8,128)} %get-tuple-element.332, f32[8,256]{1,0:T(8,128)S(1)} %bitcast.237, f32[1,8,256,64]{2,3,1,0:T(8,128)} %get-tuple-element.384, bf16[8,2048,1,64]{1,3,2,0:T(8,128)(2,1)} %get-tuple-element.396, s32[]{:T(128)} %get-tuple-element.381, ...), kind=kOutput, calls=%fused_computation.9.clone.1 | convolution fusion | flops 549847040 | bytes 18104832 | tf_op jit(solution)/shard_map/while/body/eval_jaxpr/hgqk,khd->hgqd/dot_general | solution.py:89
  198.8 8.9 %fusion.115 = f32[8,256]{1,0:T(8,128)S(1)} fusion(f32[2048,256,8]{1,0,2:T(8,128)} %get-tuple-element.332, f32[8,256]{1,0:T(8,128)S(1)} %bitcast.238), kind=kLoop, calls=%fused_computation.5.clone.1 | loop fusion | flops 12580864 | bytes 16793600 | tf_op jit(solution)/shard_map/while/body/eval_jaxpr/reduce_sum | solution.py:88
  207.8 9.0 %bitcast_reduce_fusion.6 = (f32[8,256]{1,0:T(8,128)S(1)}, f32[2048,256,8]{1,0,2:T(8,128)}) fusion(bf16[256,1,8,64]{0,3,2,1:T(8,128)(2,1)S(1)} %get-tuple-element.395, bf16[8,2048,1,64]{1,3,2,0:T(8,128)(2,1)} %get-tuple-element.394, s32[]{:T(128)} %get-tuple-element.381), kind=kOutput, calls=%fused_computation.2.clone.1 | convolution fusion | flops 545257472 | bytes 17310208 | tf_op jit(solution)/shard_map/while/body/eval_jaxpr/qhgd,khd->hgqk/dot_general | solution.py:82
  216.8 10.0 %fusion.116 = f32[1,8,256,64]{2,3,1,0:T(8,128)} fusion(f32[2048,256,8]{1,0,2:T(8,128)} %get-tuple-element.332, f32[8,256]{1,0:T(8,128)S(1)} %bitcast.237, f32[1,8,256,64]{2,3,1,0:T(8,128)} %get-tuple-element.384, bf16[8,2048,1,64]{1,3,2,0:T(8,128)(2,1)} %get-tuple-element.396, s32[]{:T(128)} %get-tuple-element.381, ...), kind=kOutput, calls=%fused_computation.9.clone.1 | convolution fusion | flops 549847040 | bytes 18104832 | tf_op jit(solution)/shard_map/while/body/eval_jaxpr/hgqk,khd->hgqd/dot_general | solution.py:89
  226.8 8.6 %fusion.115 = f32[8,256]{1,0:T(8,128)S(1)} fusion(f32[2048,256,8]{1,0,2:T(8,128)} %get-tuple-element.332, f32[8,256]{1,0:T(8,128)S(1)} %bitcast.238), kind=kLoop, calls=%fused_computation.5.clone.1 | loop fusion | flops 12580864 | bytes 16793600 | tf_op jit(solution)/shard_map/while/body/eval_jaxpr/reduce_sum | solution.py:88
  235.4 9.0 %bitcast_reduce_fusion.6 = (f32[8,256]{1,0:T(8,128)S(1)}, f32[2048,256,8]{1,0,2:T(8,128)}) fusion(bf16[256,1,8,64]{0,3,2,1:T(8,128)(2,1)S(1)} %get-tuple-element.395, bf16[8,2048,1,64]{1,3,2,0:T(8,128)(2,1)} %get-tuple-element.394, s32[]{:T(128)} %get-tuple-element.381), kind=kOutput, calls=%fused_computation.2.clone.1 | convolution fusion | flops 545257472 | bytes 17310208 | tf_op jit(solution)/shard_map/while/body/eval_jaxpr/qhgd,khd->hgqk/dot_general | solution.py:82
  244.5 9.7 %fusion.116 = f32[1,8,256,64]{2,3,1,0:T(8,128)} fusion(f32[2048,256,8]{1,0,2:T(8,128)} %get-tuple-element.332, f32[8,256]{1,0:T(8,128)S(1)} %bitcast.237, f32[1,8,256,64]{2,3,1,0:T(8,128)} %get-tuple-element.384, bf16[8,2048,1,64]{1,3,2,0:T(8,128)(2,1)} %get-tuple-element.396, s32[]{:T(128)} %get-tuple-element.381, ...), kind=kOutput, calls=%fused_computation.9.clone.1 | convolution fusion | flops 549847040 | bytes 18104832 | tf_op jit(solution)/shard_map/while/body/eval_jaxpr/hgqk,khd->hgqd/dot_general | solution.py:89
  254.1 8.6 %fusion.115 = f32[8,256]{1,0:T(8,128)S(1)} fusion(f32[2048,256,8]{1,0,2:T(8,128)} %get-tuple-element.332, f32[8,256]{1,0:T(8,128)S(1)} %bitcast.238), kind=kLoop, calls=%fused_computation.5.clone.1 | loop fusion | flops 12580864 | bytes 16793600 | tf_op jit(solution)/shard_map/while/body/eval_jaxpr/reduce_sum | solution.py:88
  262.8 9.1 %bitcast_reduce_fusion.6 = (f32[8,256]{1,0:T(8,128)S(1)}, f32[2048,256,8]{1,0,2:T(8,128)}) fusion(bf16[256,1,8,64]{0,3,2,1:T(8,128)(2,1)S(1)} %get-tuple-element.395, bf16[8,2048,1,64]{1,3,2,0:T(8,128)(2,1)} %get-tuple-element.394, s32[]{:T(128)} %get-tuple-element.381), kind=kOutput, calls=%fused_computation.2.clone.1 | convolution fusion | flops 545257472 | bytes 17310208 | tf_op jit(solution)/shard_map/while/body/eval_jaxpr/qhgd,khd->hgqk/dot_general | solution.py:82
  271.9 9.7 %fusion.116 = f32[1,8,256,64]{2,3,1,0:T(8,128)} fusion(f32[2048,256,8]{1,0,2:T(8,128)} %get-tuple-element.332, f32[8,256]{1,0:T(8,128)S(1)} %bitcast.237, f32[1,8,256,64]{2,3,1,0:T(8,128)} %get-tuple-element.384, bf16[8,2048,1,64]{1,3,2,0:T(8,128)(2,1)} %get-tuple-element.396, s32[]{:T(128)} %get-tuple-element.381, ...), kind=kOutput, calls=%fused_computation.9.clone.1 | convolution fusion | flops 549847040 | bytes 18104832 | tf_op jit(solution)/shard_map/while/body/eval_jaxpr/hgqk,khd->hgqd/dot_general | solution.py:89
  281.5 8.9 %fusion.115 = f32[8,256]{1,0:T(8,128)S(1)} fusion(f32[2048,256,8]{1,0,2:T(8,128)} %get-tuple-element.332, f32[8,256]{1,0:T(8,128)S(1)} %bitcast.238), kind=kLoop, calls=%fused_computation.5.clone.1 | loop fusion | flops 12580864 | bytes 16793600 | tf_op jit(solution)/shard_map/while/body/eval_jaxpr/reduce_sum | solution.py:88
  290.5 9.0 %bitcast_reduce_fusion.6 = (f32[8,256]{1,0:T(8,128)S(1)}, f32[2048,256,8]{1,0,2:T(8,128)}) fusion(bf16[256,1,8,64]{0,3,2,1:T(8,128)(2,1)S(1)} %get-tuple-element.395, bf16[8,2048,1,64]{1,3,2,0:T(8,128)(2,1)} %get-tuple-element.394, s32[]{:T(128)} %get-tuple-element.381), kind=kOutput, calls=%fused_computation.2.clone.1 | convolution fusion | flops 545257472 | bytes 17310208 | tf_op jit(solution)/shard_map/while/body/eval_jaxpr/qhgd,khd->hgqk/dot_general | solution.py:82
  299.6 9.7 %fusion.116 = f32[1,8,256,64]{2,3,1,0:T(8,128)} fusion(f32[2048,256,8]{1,0,2:T(8,128)} %get-tuple-element.332, f32[8,256]{1,0:T(8,128)S(1)} %bitcast.237, f32[1,8,256,64]{2,3,1,0:T(8,128)} %get-tuple-element.384, bf16[8,2048,1,64]{1,3,2,0:T(8,128)(2,1)} %get-tuple-element.396, s32[]{:T(128)} %get-tuple-element.381, ...), kind=kOutput, calls=%fused_computation.9.clone.1 | convolution fusion | flops 549847040 | bytes 18104832 | tf_op jit(solution)/shard_map/while/body/eval_jaxpr/hgqk,khd->hgqd/dot_general | solution.py:89
  309.2 8.6 %fusion.115 = f32[8,256]{1,0:T(8,128)S(1)} fusion(f32[2048,256,8]{1,0,2:T(8,128)} %get-tuple-element.332, f32[8,256]{1,0:T(8,128)S(1)} %bitcast.238), kind=kLoop, calls=%fused_computation.5.clone.1 | loop fusion | flops 12580864 | bytes 16793600 | tf_op jit(solution)/shard_map/while/body/eval_jaxpr/reduce_sum | solution.py:88
  317.8 9.0 %bitcast_reduce_fusion.6 = (f32[8,256]{1,0:T(8,128)S(1)}, f32[2048,256,8]{1,0,2:T(8,128)}) fusion(bf16[256,1,8,64]{0,3,2,1:T(8,128)(2,1)S(1)} %get-tuple-element.395, bf16[8,2048,1,64]{1,3,2,0:T(8,128)(2,1)} %get-tuple-element.394, s32[]{:T(128)} %get-tuple-element.381), kind=kOutput, calls=%fused_computation.2.clone.1 | convolution fusion | flops 545257472 | bytes 17310208 | tf_op jit(solution)/shard_map/while/body/eval_jaxpr/qhgd,khd->hgqk/dot_general | solution.py:82
  326.9 9.7 %fusion.116 = f32[1,8,256,64]{2,3,1,0:T(8,128)} fusion(f32[2048,256,8]{1,0,2:T(8,128)} %get-tuple-element.332, f32[8,256]{1,0:T(8,128)S(1)} %bitcast.237, f32[1,8,256,64]{2,3,1,0:T(8,128)} %get-tuple-element.384, bf16[8,2048,1,64]{1,3,2,0:T(8,128)(2,1)} %get-tuple-element.396, s32[]{:T(128)} %get-tuple-element.381, ...), kind=kOutput, calls=%fused_computation.9.clone.1 | convolution fusion | flops 549847040 | bytes 18104832 | tf_op jit(solution)/shard_map/while/body/eval_jaxpr/hgqk,khd->hgqd/dot_general | solution.py:89
  336.5 8.6 %fusion.115 = f32[8,256]{1,0:T(8,128)S(1)} fusion(f32[2048,256,8]{1,0,2:T(8,128)} %get-tuple-element.332, f32[8,256]{1,0:T(8,128)S(1)} %bitcast.238), kind=kLoop, calls=%fused_computation.5.clone.1 | loop fusion | flops 12580864 | bytes 16793600 | tf_op jit(solution)/shard_map/while/body/eval_jaxpr/reduce_sum | solution.py:88
  345.1 9.0 %bitcast_reduce_fusion.6 = (f32[8,256]{1,0:T(8,128)S(1)}, f32[2048,256,8]{1,0,2:T(8,128)}) fusion(bf16[256,1,8,64]{0,3,2,1:T(8,128)(2,1)S(1)} %get-tuple-element.395, bf16[8,2048,1,64]{1,3,2,0:T(8,128)(2,1)} %get-tuple-element.394, s32[]{:T(128)} %get-tuple-element.381), kind=kOutput, calls=%fused_computation.2.clone.1 | convolution fusion | flops 545257472 | bytes 17310208 | tf_op jit(solution)/shard_map/while/body/eval_jaxpr/qhgd,khd->hgqk/dot_general | solution.py:82
  354.2 9.7 %fusion.116 = f32[1,8,256,64]{2,3,1,0:T(8,128)} fusion(f32[2048,256,8]{1,0,2:T(8,128)} %get-tuple-element.332, f32[8,256]{1,0:T(8,128)S(1)} %bitcast.237, f32[1,8,256,64]{2,3,1,0:T(8,128)} %get-tuple-element.384, bf16[8,2048,1,64]{1,3,2,0:T(8,128)(2,1)} %get-tuple-element.396, s32[]{:T(128)} %get-tuple-element.381, ...), kind=kOutput, calls=%fused_computation.9.clone.1 | convolution fusion | flops 549847040 | bytes 18104832 | tf_op jit(solution)/shard_map/while/body/eval_jaxpr/hgqk,khd->hgqd/dot_general | solution.py:89
  363.8 8.6 %fusion.115 = f32[8,256]{1,0:T(8,128)S(1)} fusion(f32[2048,256,8]{1,0,2:T(8,128)} %get-tuple-element.332, f32[8,256]{1,0:T(8,128)S(1)} %bitcast.238), kind=kLoop, calls=%fused_computation.5.clone.1 | loop fusion | flops 12580864 | bytes 16793600 | tf_op jit(solution)/shard_map/while/body/eval_jaxpr/reduce_sum | solution.py:88
  380.6 103.4 %while.31 = (s32[]{:T(128)}, f32[1,4,256]{2,1,0:T(4,128)S(1)}, f32[1,4,256]{2,1,0:T(4,128)S(1)}, f32[1,4,256,128]{3,2,1,0:T(8,128)S(1)}, bf16[8,2048,1,128]{3,1,...) while((s32[]{:T(128)}, f32[1,4,256]{2,1,0:T(4,128)S(1)}, ...), condition=%wide.region_11.12_spmd.clone, body=%wide.region_8.11_spmd.clone.sunk | while | flops 1090918400 | bytes 61146240 | solution.py:107
  493.8 38.3 %all_to_all.26 = bf16[64,8,2048]{2,1,0:T(8,128)(2,1)S(1)} all-to-all(bf16[64,8,2048]{2,1,0:T(8,128)(2,1)S(1)} %fusion.48), channel_id=1, replica_groups=mesh['sp'=64,'tp'=2] {'sp'}, dimensions={0} | all-to-all | bytes 4194304 | tf_op jit(solution)/shard_map/all_to_all | solution.py:202
  545.8 10.0 %convolution_convert_fusion = bf16[1024,2048]{1,0:T(8,128)(2,1)} fusion(bf16[1,512,2048]{2,1,0:T(8,128)(2,1)S(1)} %copy-done, f32[1024,512]{1,0:T(8,128)} %fusion.53, bf16[1024,2048]{1,0:T(8,128)(2,1)} %bitcast.240, bf16[1,2048,512]{2,1,0:T(8,128)(2,1)} %param.35), kind=kOutput, calls=%fused_computation.53 | convolution fusion | flops 4300210176 | bytes 14680064 | tf_op jit(solution)/shard_map/dot_general | solution.py:208
  555.8 11.9 %all_to_all.28 = bf16[2,64,8,2048]{3,2,1,0:T(8,128)(2,1)} all-to-all(bf16[2,64,8,2048]{3,2,1,0:T(8,128)(2,1)} %bitcast.241), channel_id=1, replica_groups=mesh['sp'=64,'tp'=2] {'tp'}, dimensions={0} | all-to-all | bytes 8388608 | tf_op jit(solution)/shard_map/all_to_all | solution.py:22
  579.5 29.6 %all-to-all-done.4 = bf16[64,8,2048]{2,1,0:T(8,128)(2,1)} async-done(((bf16[64,8,2048]{2,1,0:T(8,128)(2,1)}), bf16[64,8,2048]{2,1,0:T(8,128)(2,1)}, u32[]{:S(2)}, u32[]{:S(2)}) %all-to-all-start.4) | async-done | bytes 2097184 | tf_op jit(solution)/shard_map/all_to_all | solution.py:213
  (203 shorter events, 189.9 us)
Async XLA Ops:
  6.5 539.2 %copy-start = (bf16[1,512,2048]{2,1,0:T(8,128)(2,1)S(1)}, bf16[1,512,2048]{2,1,0:T(8,128)(2,1)}, u32[]{:S(2)}) copy-start(bf16[1,512,2048]{2,1,0:T(8,128)(2,1)} %param.37) | copy-start | bytes 6291460
  6.5 13.6 %copy-start.6 = (s32[128,2]{0,1:T(2,128)S(1)}, s32[128,2]{0,1:T(2,128)}, u32[]{:S(2)}) copy-start(s32[128,2]{0,1:T(2,128)} %param.38) | copy-start | bytes 3076
  6.5 72.4 %all-gather.5.cloned.1.call-start = ((), (), s32[]{:S(2)}) async-start(), calls=%async_computation.5 | async-start | bytes 2129920 | tf_op jit(solution)/shard_map/all_gather | solution.py:159
  9.2 138.0 %all-gather.7.cloned.1.call-start = ((), (), s32[]{:S(2)}) async-start(), calls=%async_computation.6 | async-start | bytes 2129920 | tf_op jit(solution)/shard_map/all_gather | solution.py:160
  9.9 364.3 %all-gather.9.cloned.1.call-start = ((), (), s32[]{:S(2)}) async-start(), calls=%async_computation.7 | async-start | bytes 4259840 | tf_op jit(solution)/shard_map/all_gather | solution.py:161
  12.7 367.8 %all-gather.11.cloned.1.call-start = ((), (), s32[]{:S(2)}) async-start(), calls=%async_computation.8 | async-start | bytes 4259840 | tf_op jit(solution)/shard_map/all_gather | solution.py:162
  19.9 0.8 copy-start.4
  386.6 5.9 copy-start.1
  399.5 5.9 copy-start.1
  412.3 5.9 copy-start.1
  425.2 5.9 copy-start.1
  438.1 5.9 copy-start.1
  450.9 5.9 copy-start.1
  463.8 5.9 copy-start.1
  476.7 5.9 copy-start.1
  487.8 4.9 copy-start.3
  487.8 5.2 copy-start.8
  532.7 9.4 %copy-start.11 = (bf16[1,2048,512]{2,1,0:T(8,128)(2,1)S(1)}, bf16[1,2048,512]{2,1,0:T(8,128)(2,1)}, u32[]{:S(2)}) copy-start(bf16[1,2048,512]{2,1,0:T(8,128)(2,1)} %param.36) | copy-start | bytes 6291460
  540.1 2.0 copy-start.2
  567.7 11.3 %copy-start.7 = (s32[128,2]{0,1:T(2,128)S(1)}, s32[128,2]{0,1:T(2,128)}, u32[]{:S(2)}) copy-start(s32[128,2]{0,1:T(2,128)} %param.38) | copy-start | bytes 3076
  567.7 11.5 %copy-start.9 = (pred[128,2]{0,1:T(4,128)(4,1)S(1)}, pred[128,2]{0,1:T(4,128)(4,1)}, u32[]{:S(2)}) copy-start(pred[128,2]{0,1:T(4,128)(4,1)} %get-tuple-element.207) | copy-start | bytes 772
  567.7 11.7 %copy-start.10 = (f32[128,2]{0,1:T(2,128)S(1)}, f32[128,2]{0,1:T(2,128)}, u32[]{:S(2)}) copy-start(f32[128,2]{0,1:T(2,128)} %param.39) | copy-start | bytes 3076
  567.7 11.8 %copy-start.5 = (s32[256]{0:T(256)S(1)}, s32[256]{0:T(256)}, u32[]{:S(2)}) copy-start(s32[256]{0:T(256)} %copy-done.4) | copy-start | bytes 3076
  572.7 36.4 %all-to-all-start.4 = ((bf16[64,8,2048]{2,1,0:T(8,128)(2,1)}), bf16[64,8,2048]{2,1,0:T(8,128)(2,1)}, u32[]{:S(2)}, u32[]{:S(2)}) async-start(bf16[64,8,2048]{2,1,0:T(8,128)(2,1)} %reduce_sum.131), calls=%async_computation.4 | async-start | bytes 4194304 | tf_op jit(solution)/shard_map/all_to_all | solution.py:213
Sparse Core Ops, SparseCore 0:
  10.0 68.8 all-gather.4
  81.6 65.5 all-gather.6
  149.9 73.9 all-gather.8
  226.7 69.3 all-gather.10
where the time goes:
time: 638 us; the launch traced here: 630 us
  matrix products  254 us (40%)
  waiting for transfers between devices  147 us (23%)
  other arithmetic  101 us (16%)
  blocking collectives  62.3 us (10%)
  local copies, waits for them, and re-layouts  44.2 us (7%)
  between operations  13.7 us (2%)
    dot_general x16, matrix products, attend_block(): jnp.einsum('hgqk,khd->hgqd', weights.astype(jnp.bfloat16), values, prefer...  120 us
    dot_general x16, matrix products, attend_block(): jnp.einsum('qhgd,khd->hgqk', queries, keys, preferred_element_type=jnp.fl...  116 us
    reduce_sum x16, other arithmetic, attend_block(): total = total * shrink + jnp.sum(weights, axis=-1)  80.2 us
    all_gather x1, waiting for transfers between devices, local(): lax.all_gather(value_narrow, 'sp', axis=0, tiled=True)  63 us
    all_gather x1, waiting for transfers between devices, local(): lax.all_gather(keys_n, 'sp', axis=0, tiled=True)  53 us
    all_to_all x1, blocking collectives, local(): lax.all_to_all(sent, 'sp', split_axis=0, concat_axis=0, tiled=True)  38.3 us
    all_to_all x1, waiting for transfers between devices, local(): back = lax.all_to_all(summed, 'sp', split_axis=0, concat_axis=0, tiled=True)  29.6 us
    unnamed x33, local copies, waits for them, and re-layouts  23.1 us
  transfers between devices with their start and end apart: 5, of which 3 were waited for; matrix products, arithmetic and copies ran while one was open for 40% of the time, Pallas kernels for 0%

commit v1 on v0

--- a/solution.py
+++ b/solution.py
@@ -156,7 +156,9 @@
         shaped_b,
         (start_n, start_b),
         (
-            lax.all_gather(keys_n, "sp", axis=0, tiled=True),
+            jnp.concatenate(
+                lax.all_to_all(jnp.stack([keys_n] * lax.axis_size("sp")), "sp", 0, 0), axis=0
+            ),
             lax.all_gather(value_narrow, "sp", axis=0, tiled=True),
             lax.all_gather(keys_b, "sp", axis=0, tiled=True),
             lax.all_gather(value_broad, "sp", axis=0, tiled=True),

time: 638 us -> 588 us (0.922)
  waiting for transfers between devices: 147 us -> 72.7 us
  starting transfers between devices: 6.3 us -> 18 us
  local copies, waits for them, and re-layouts: 44.2 us -> 51.7 us
    all_gather x1 -> x0, waiting for transfers between devices: 53 us -> none  [local(): lax.all_gather(keys_n, 'sp', axis=0, tiled=True)]
    all_gather x1, waiting for transfers between devices: 63 us -> 26.3 us  [local(): lax.all_gather(value_narrow, 'sp', axis=0, tiled=True)]
    all_to_all x0 -> x1, waiting for transfers between devices: none -> 15.3 us  [local(): lax.all_to_all(jnp.stack([keys_n] * lax.axis_size('sp')), 'sp', 0, 0)]
    all_to_all x0 -> x1, starting transfers between devices: none -> 11.8 us  [local(): lax.all_to_all(jnp.stack([keys_n] * lax.axis_size('sp')), 'sp', 0, 0)]
    unnamed x33 -> x36, local copies, waits for them, and re-layouts: 23.1 us -> 20.3 us
  transfers between devices with their start and end apart: 5 -> 5, of which waited for: 3 -> 3; matrix products, arithmetic and copies ran while one was open for 40% -> 46% of each run, Pallas kernels for 0% -> 0%
where the time goes in v1:
time: 588 us; the launch traced here: 578 us
  matrix products  254 us (43%)
  other arithmetic  104 us (18%)
  waiting for transfers between devices  72.7 us (12%)
  blocking collectives  62.2 us (11%)
  local copies, waits for them, and re-layouts  51.7 us (9%)
  starting transfers between devices  18 us (3%)
  between operations  13.8 us (2%)
    dot_general x16, matrix products, attend_block(): jnp.einsum('hgqk,khd->hgqd', weights.astype(jnp.bfloat16), values, prefer...  120 us
    dot_general x16, matrix products, attend_block(): jnp.einsum('qhgd,khd->hgqk', queries, keys, preferred_element_type=jnp.fl...  116 us
    reduce_sum x16, other arithmetic, attend_block(): total = total * shrink + jnp.sum(weights, axis=-1)  80.2 us
    all_to_all x1, blocking collectives, local(): lax.all_to_all(sent, 'sp', split_axis=0, concat_axis=0, tiled=True)  38.3 us
    all_to_all x1, waiting for transfers between devices, local(): back = lax.all_to_all(summed, 'sp', split_axis=0, concat_axis=0, tiled=True)  29.6 us
    all_gather x1, waiting for transfers between devices, local(): lax.all_gather(value_narrow, 'sp', axis=0, tiled=True)  26.3 us
    unnamed x36, local copies, waits for them, and re-layouts  20.3 us
    all_to_all x2, blocking collectives, summed_on_arrival(): blocks = lax.all_to_all(cut_along(value, dim, size), axis, 0, 0, tiled=True)  16.6 us
  transfers between devices with their start and end apart: 5, of which 3 were waited for; matrix products, arithmetic and copies ran while one was open for 46% of the time, Pallas kernels for 0%

profile of v1, /device:TPU:0, one launch (start us, length us, event | category | flops | bytes accessed | tf_op | source)
XLA Modules:
  0.0 578.2 jit_solution(6420926640544396844)
XLA Ops:
  14.7 11.8 %all-to-all-start = ((bf16[64,256,64]{1,2,0:T(8,128)(2,1)}), bf16[64,256,64]{1,2,0:T(8,128)(2,1)}, u32[]{:S(2)}, u32[]{:S(2)}) async-start(bf16[64,256,64]{1,2,0:T(8,128)(2,1)} %stack.34), calls=%async_computation | async-start | bytes 4194304 | tf_op jit(solution)/shard_map/all_to_all | solution.py:160
  41.4 15.3 %all-to-all-done = bf16[64,256,64]{1,2,0:T(8,128)(2,1)} async-done(((bf16[64,256,64]{1,2,0:T(8,128)(2,1)}), bf16[64,256,64]{1,2,0:T(8,128)(2,1)}, u32[]{:S(2)}, u32[]{:S(2)}) %all-to-all-start) | async-done | bytes 2097184 | tf_op jit(solution)/shard_map/all_to_all | solution.py:160
  69.1 26.3 %all-gather.4.cloned.1.call-done = bf16[16384,64]{0,1:T(8,128)(2,1)} async-done(((bf16[256,64]{0,1:T(8,128)(2,1)}), bf16[16384,64]{0,1:T(8,128)(2,1)}) %all-gather.4.cloned.1.call-update) | async-done | bytes 2097168 | tf_op jit(solution)/shard_map/all_gather | solution.py:162
  100.7 219.9 %while.30 = (s32[]{:T(128)}, f32[1,8,256]{2,1,0:T(8,128)S(1)}, f32[1,8,256]{2,1,0:T(8,128)S(1)}, f32[1,8,256,64]{2,3,1,0:T(8,128)}, bf16[8,2048,1,64]{1,3,2,0:T(...) while((s32[]{:T(128)}, f32[1,8,256]{2,1,0:T(8,128)S(1)}, ...), condition=%wide.region_5.6_spmd.clone, body=%wide.region_2.5_spmd.clone.sunk | while | flops 1107701760 | bytes 52298852 | solution.py:107
  101.0 9.0 %bitcast_reduce_fusion.6 = (f32[8,256]{1,0:T(8,128)S(1)}, f32[2048,256,8]{1,0,2:T(8,128)}) fusion(bf16[256,1,8,64]{0,3,2,1:T(8,128)(2,1)S(1)} %get-tuple-element.409, bf16[8,2048,1,64]{1,3,2,0:T(8,128)(2,1)} %get-tuple-element.408, s32[]{:T(128)} %get-tuple-element.395), kind=kOutput, calls=%fused_computation.2.clone.1 | convolution fusion | flops 545257472 | bytes 17310208 | tf_op jit(solution)/shard_map/while/body/eval_jaxpr/qhgd,khd->hgqk/dot_general | solution.py:82
  110.0 9.6 %fusion.116 = f32[1,8,256,64]{2,3,1,0:T(8,128)} fusion(f32[2048,256,8]{1,0,2:T(8,128)} %get-tuple-element.346, f32[8,256]{1,0:T(8,128)S(1)} %bitcast.233, f32[1,8,256,64]{2,3,1,0:T(8,128)} %get-tuple-element.398, bf16[8,2048,1,64]{1,3,2,0:T(8,128)(2,1)} %get-tuple-element.410, s32[]{:T(128)} %get-tuple-element.395, ...), kind=kOutput, calls=%fused_computation.9.clone.1 | convolution fusion | flops 549847040 | bytes 18104832 | tf_op jit(solution)/shard_map/while/body/eval_jaxpr/hgqk,khd->hgqd/dot_general | solution.py:89
  119.7 8.6 %fusion.115 = f32[8,256]{1,0:T(8,128)S(1)} fusion(f32[2048,256,8]{1,0,2:T(8,128)} %get-tuple-element.346, f32[8,256]{1,0:T(8,128)S(1)} %bitcast.234), kind=kLoop, calls=%fused_computation.5.clone.1 | loop fusion | flops 12580864 | bytes 16793600 | tf_op jit(solution)/shard_map/while/body/eval_jaxpr/reduce_sum | solution.py:88
  128.3 9.0 %bitcast_reduce_fusion.6 = (f32[8,256]{1,0:T(8,128)S(1)}, f32[2048,256,8]{1,0,2:T(8,128)}) fusion(bf16[256,1,8,64]{0,3,2,1:T(8,128)(2,1)S(1)} %get-tuple-element.409, bf16[8,2048,1,64]{1,3,2,0:T(8,128)(2,1)} %get-tuple-element.408, s32[]{:T(128)} %get-tuple-element.395), kind=kOutput, calls=%fused_computation.2.clone.1 | convolution fusion | flops 545257472 | bytes 17310208 | tf_op jit(solution)/shard_map/while/body/eval_jaxpr/qhgd,khd->hgqk/dot_general | solution.py:82
  137.3 9.7 %fusion.116 = f32[1,8,256,64]{2,3,1,0:T(8,128)} fusion(f32[2048,256,8]{1,0,2:T(8,128)} %get-tuple-element.346, f32[8,256]{1,0:T(8,128)S(1)} %bitcast.233, f32[1,8,256,64]{2,3,1,0:T(8,128)} %get-tuple-element.398, bf16[8,2048,1,64]{1,3,2,0:T(8,128)(2,1)} %get-tuple-element.410, s32[]{:T(128)} %get-tuple-element.395, ...), kind=kOutput, calls=%fused_computation.9.clone.1 | convolution fusion | flops 549847040 | bytes 18104832 | tf_op jit(solution)/shard_map/while/body/eval_jaxpr/hgqk,khd->hgqd/dot_general | solution.py:89
  147.0 8.9 %fusion.115 = f32[8,256]{1,0:T(8,128)S(1)} fusion(f32[2048,256,8]{1,0,2:T(8,128)} %get-tuple-element.346, f32[8,256]{1,0:T(8,128)S(1)} %bitcast.234), kind=kLoop, calls=%fused_computation.5.clone.1 | loop fusion | flops 12580864 | bytes 16793600 | tf_op jit(solution)/shard_map/while/body/eval_jaxpr/reduce_sum | solution.py:88
  156.0 9.0 %bitcast_reduce_fusion.6 = (f32[8,256]{1,0:T(8,128)S(1)}, f32[2048,256,8]{1,0,2:T(8,128)}) fusion(bf16[256,1,8,64]{0,3,2,1:T(8,128)(2,1)S(1)} %get-tuple-element.409, bf16[8,2048,1,64]{1,3,2,0:T(8,128)(2,1)} %get-tuple-element.408, s32[]{:T(128)} %get-tuple-element.395), kind=kOutput, calls=%fused_computation.2.clone.1 | convolution fusion | flops 545257472 | bytes 17310208 | tf_op jit(solution)/shard_map/while/body/eval_jaxpr/qhgd,khd->hgqk/dot_general | solution.py:82
  165.0 10.0 %fusion.116 = f32[1,8,256,64]{2,3,1,0:T(8,128)} fusion(f32[2048,256,8]{1,0,2:T(8,128)} %get-tuple-element.346, f32[8,256]{1,0:T(8,128)S(1)} %bitcast.233, f32[1,8,256,64]{2,3,1,0:T(8,128)} %get-tuple-element.398, bf16[8,2048,1,64]{1,3,2,0:T(8,128)(2,1)} %get-tuple-element.410, s32[]{:T(128)} %get-tuple-element.395, ...), kind=kOutput, calls=%fused_computation.9.clone.1 | convolution fusion | flops 549847040 | bytes 18104832 | tf_op jit(solution)/shard_map/while/body/eval_jaxpr/hgqk,khd->hgqd/dot_general | solution.py:89
  175.0 8.6 %fusion.115 = f32[8,256]{1,0:T(8,128)S(1)} fusion(f32[2048,256,8]{1,0,2:T(8,128)} %get-tuple-element.346, f32[8,256]{1,0:T(8,128)S(1)} %bitcast.234), kind=kLoop, calls=%fused_computation.5.clone.1 | loop fusion | flops 12580864 | bytes 16793600 | tf_op jit(solution)/shard_map/while/body/eval_jaxpr/reduce_sum | solution.py:88
  183.6 9.0 %bitcast_reduce_fusion.6 = (f32[8,256]{1,0:T(8,128)S(1)}, f32[2048,256,8]{1,0,2:T(8,128)}) fusion(bf16[256,1,8,64]{0,3,2,1:T(8,128)(2,1)S(1)} %get-tuple-element.409, bf16[8,2048,1,64]{1,3,2,0:T(8,128)(2,1)} %get-tuple-element.408, s32[]{:T(128)} %get-tuple-element.395), kind=kOutput, calls=%fused_computation.2.clone.1 | convolution fusion | flops 545257472 | bytes 17310208 | tf_op jit(solution)/shard_map/while/body/eval_jaxpr/qhgd,khd->hgqk/dot_general | solution.py:82
  192.7 9.7 %fusion.116 = f32[1,8,256,64]{2,3,1,0:T(8,128)} fusion(f32[2048,256,8]{1,0,2:T(8,128)} %get-tuple-element.346, f32[8,256]{1,0:T(8,128)S(1)} %bitcast.233, f32[1,8,256,64]{2,3,1,0:T(8,128)} %get-tuple-element.398, bf16[8,2048,1,64]{1,3,2,0:T(8,128)(2,1)} %get-tuple-element.410, s32[]{:T(128)} %get-tuple-element.395, ...), kind=kOutput, calls=%fused_computation.9.clone.1 | convolution fusion | flops 549847040 | bytes 18104832 | tf_op jit(solution)/shard_map/while/body/eval_jaxpr/hgqk,khd->hgqd/dot_general | solution.py:89
  202.3 8.6 %fusion.115 = f32[8,256]{1,0:T(8,128)S(1)} fusion(f32[2048,256,8]{1,0,2:T(8,128)} %get-tuple-element.346, f32[8,256]{1,0:T(8,128)S(1)} %bitcast.234), kind=kLoop, calls=%fused_computation.5.clone.1 | loop fusion | flops 12580864 | bytes 16793600 | tf_op jit(solution)/shard_map/while/body/eval_jaxpr/reduce_sum | solution.py:88
  211.0 9.1 %bitcast_reduce_fusion.6 = (f32[8,256]{1,0:T(8,128)S(1)}, f32[2048,256,8]{1,0,2:T(8,128)}) fusion(bf16[256,1,8,64]{0,3,2,1:T(8,128)(2,1)S(1)} %get-tuple-element.409, bf16[8,2048,1,64]{1,3,2,0:T(8,128)(2,1)} %get-tuple-element.408, s32[]{:T(128)} %get-tuple-element.395), kind=kOutput, calls=%fused_computation.2.clone.1 | convolution fusion | flops 545257472 | bytes 17310208 | tf_op jit(solution)/shard_map/while/body/eval_jaxpr/qhgd,khd->hgqk/dot_general | solution.py:82
  220.1 9.7 %fusion.116 = f32[1,8,256,64]{2,3,1,0:T(8,128)} fusion(f32[2048,256,8]{1,0,2:T(8,128)} %get-tuple-element.346, f32[8,256]{1,0:T(8,128)S(1)} %bitcast.233, f32[1,8,256,64]{2,3,1,0:T(8,128)} %get-tuple-element.398, bf16[8,2048,1,64]{1,3,2,0:T(8,128)(2,1)} %get-tuple-element.410, s32[]{:T(128)} %get-tuple-element.395, ...), kind=kOutput, calls=%fused_computation.9.clone.1 | convolution fusion | flops 549847040 | bytes 18104832 | tf_op jit(solution)/shard_map/while/body/eval_jaxpr/hgqk,khd->hgqd/dot_general | solution.py:89
  229.7 8.9 %fusion.115 = f32[8,256]{1,0:T(8,128)S(1)} fusion(f32[2048,256,8]{1,0,2:T(8,128)} %get-tuple-element.346, f32[8,256]{1,0:T(8,128)S(1)} %bitcast.234), kind=kLoop, calls=%fused_computation.5.clone.1 | loop fusion | flops 12580864 | bytes 16793600 | tf_op jit(solution)/shard_map/while/body/eval_jaxpr/reduce_sum | solution.py:88
  238.7 9.0 %bitcast_reduce_fusion.6 = (f32[8,256]{1,0:T(8,128)S(1)}, f32[2048,256,8]{1,0,2:T(8,128)}) fusion(bf16[256,1,8,64]{0,3,2,1:T(8,128)(2,1)S(1)} %get-tuple-element.409, bf16[8,2048,1,64]{1,3,2,0:T(8,128)(2,1)} %get-tuple-element.408, s32[]{:T(128)} %get-tuple-element.395), kind=kOutput, calls=%fused_computation.2.clone.1 | convolution fusion | flops 545257472 | bytes 17310208 | tf_op jit(solution)/shard_map/while/body/eval_jaxpr/qhgd,khd->hgqk/dot_general | solution.py:82
  247.8 9.7 %fusion.116 = f32[1,8,256,64]{2,3,1,0:T(8,128)} fusion(f32[2048,256,8]{1,0,2:T(8,128)} %get-tuple-element.346, f32[8,256]{1,0:T(8,128)S(1)} %bitcast.233, f32[1,8,256,64]{2,3,1,0:T(8,128)} %get-tuple-element.398, bf16[8,2048,1,64]{1,3,2,0:T(8,128)(2,1)} %get-tuple-element.410, s32[]{:T(128)} %get-tuple-element.395, ...), kind=kOutput, calls=%fused_computation.9.clone.1 | convolution fusion | flops 549847040 | bytes 18104832 | tf_op jit(solution)/shard_map/while/body/eval_jaxpr/hgqk,khd->hgqd/dot_general | solution.py:89
  257.4 8.6 %fusion.115 = f32[8,256]{1,0:T(8,128)S(1)} fusion(f32[2048,256,8]{1,0,2:T(8,128)} %get-tuple-element.346, f32[8,256]{1,0:T(8,128)S(1)} %bitcast.234), kind=kLoop, calls=%fused_computation.5.clone.1 | loop fusion | flops 12580864 | bytes 16793600 | tf_op jit(solution)/shard_map/while/body/eval_jaxpr/reduce_sum | solution.py:88
  266.0 9.0 %bitcast_reduce_fusion.6 = (f32[8,256]{1,0:T(8,128)S(1)}, f32[2048,256,8]{1,0,2:T(8,128)}) fusion(bf16[256,1,8,64]{0,3,2,1:T(8,128)(2,1)S(1)} %get-tuple-element.409, bf16[8,2048,1,64]{1,3,2,0:T(8,128)(2,1)} %get-tuple-element.408, s32[]{:T(128)} %get-tuple-element.395), kind=kOutput, calls=%fused_computation.2.clone.1 | convolution fusion | flops 545257472 | bytes 17310208 | tf_op jit(solution)/shard_map/while/body/eval_jaxpr/qhgd,khd->hgqk/dot_general | solution.py:82
  275.1 9.7 %fusion.116 = f32[1,8,256,64]{2,3,1,0:T(8,128)} fusion(f32[2048,256,8]{1,0,2:T(8,128)} %get-tuple-element.346, f32[8,256]{1,0:T(8,128)S(1)} %bitcast.233, f32[1,8,256,64]{2,3,1,0:T(8,128)} %get-tuple-element.398, bf16[8,2048,1,64]{1,3,2,0:T(8,128)(2,1)} %get-tuple-element.410, s32[]{:T(128)} %get-tuple-element.395, ...), kind=kOutput, calls=%fused_computation.9.clone.1 | convolution fusion | flops 549847040 | bytes 18104832 | tf_op jit(solution)/shard_map/while/body/eval_jaxpr/hgqk,khd->hgqd/dot_general | solution.py:89
  284.7 8.6 %fusion.115 = f32[8,256]{1,0:T(8,128)S(1)} fusion(f32[2048,256,8]{1,0,2:T(8,128)} %get-tuple-element.346, f32[8,256]{1,0:T(8,128)S(1)} %bitcast.234), kind=kLoop, calls=%fused_computation.5.clone.1 | loop fusion | flops 12580864 | bytes 16793600 | tf_op jit(solution)/shard_map/while/body/eval_jaxpr/reduce_sum | solution.py:88
  293.3 9.0 %bitcast_reduce_fusion.6 = (f32[8,256]{1,0:T(8,128)S(1)}, f32[2048,256,8]{1,0,2:T(8,128)}) fusion(bf16[256,1,8,64]{0,3,2,1:T(8,128)(2,1)S(1)} %get-tuple-element.409, bf16[8,2048,1,64]{1,3,2,0:T(8,128)(2,1)} %get-tuple-element.408, s32[]{:T(128)} %get-tuple-element.395), kind=kOutput, calls=%fused_computation.2.clone.1 | convolution fusion | flops 545257472 | bytes 17310208 | tf_op jit(solution)/shard_map/while/body/eval_jaxpr/qhgd,khd->hgqk/dot_general | solution.py:82
  302.4 9.7 %fusion.116 = f32[1,8,256,64]{2,3,1,0:T(8,128)} fusion(f32[2048,256,8]{1,0,2:T(8,128)} %get-tuple-element.346, f32[8,256]{1,0:T(8,128)S(1)} %bitcast.233, f32[1,8,256,64]{2,3,1,0:T(8,128)} %get-tuple-element.398, bf16[8,2048,1,64]{1,3,2,0:T(8,128)(2,1)} %get-tuple-element.410, s32[]{:T(128)} %get-tuple-element.395, ...), kind=kOutput, calls=%fused_computation.9.clone.1 | convolution fusion | flops 549847040 | bytes 18104832 | tf_op jit(solution)/shard_map/while/body/eval_jaxpr/hgqk,khd->hgqd/dot_general | solution.py:89
  328.8 103.4 %while.31 = (s32[]{:T(128)}, f32[1,4,256]{2,1,0:T(4,128)S(1)}, f32[1,4,256]{2,1,0:T(4,128)S(1)}, f32[1,4,256,128]{3,2,1,0:T(8,128)S(1)}, bf16[8,2048,1,128]{3,1,...) while((s32[]{:T(128)}, f32[1,4,256]{2,1,0:T(4,128)S(1)}, ...), condition=%wide.region_11.12_spmd.clone, body=%wide.region_8.11_spmd.clone.sunk | while | flops 1090918400 | bytes 61146240 | solution.py:107
  442.0 38.3 %all_to_all.31 = bf16[64,8,2048]{2,1,0:T(8,128)(2,1)S(1)} all-to-all(bf16[64,8,2048]{2,1,0:T(8,128)(2,1)S(1)} %fusion.48), channel_id=1, replica_groups=mesh['sp'=64,'tp'=2] {'sp'}, dimensions={0} | all-to-all | bytes 4194304 | tf_op jit(solution)/shard_map/all_to_all | solution.py:204
  493.9 10.1 %convolution_convert_fusion = bf16[1024,2048]{1,0:T(8,128)(2,1)} fusion(bf16[1,512,2048]{2,1,0:T(8,128)(2,1)S(1)} %copy-done, f32[1024,512]{1,0:T(8,128)} %fusion.53, bf16[1024,2048]{1,0:T(8,128)(2,1)} %bitcast.236, bf16[1,2048,512]{2,1,0:T(8,128)(2,1)} %param.35), kind=kOutput, calls=%fused_computation.53 | convolution fusion | flops 4300210176 | bytes 14680064 | tf_op jit(solution)/shard_map/dot_general | solution.py:210
  504.0 11.9 %all_to_all.33 = bf16[2,64,8,2048]{3,2,1,0:T(8,128)(2,1)} all-to-all(bf16[2,64,8,2048]{3,2,1,0:T(8,128)(2,1)} %bitcast.237), channel_id=1, replica_groups=mesh['sp'=64,'tp'=2] {'tp'}, dimensions={0} | all-to-all | bytes 8388608 | tf_op jit(solution)/shard_map/all_to_all | solution.py:22
  527.7 29.6 %all-to-all-done.5 = bf16[64,8,2048]{2,1,0:T(8,128)(2,1)} async-done(((bf16[64,8,2048]{2,1,0:T(8,128)(2,1)}), bf16[64,8,2048]{2,1,0:T(8,128)(2,1)}, u32[]{:S(2)}, u32[]{:S(2)}) %all-to-all-start.5) | async-done | bytes 2097184 | tf_op jit(solution)/shard_map/all_to_all | solution.py:215
  (208 shorter events, 209.3 us)
Async XLA Ops:
  6.5 487.4 %copy-start = (bf16[1,512,2048]{2,1,0:T(8,128)(2,1)S(1)}, bf16[1,512,2048]{2,1,0:T(8,128)(2,1)}, u32[]{:S(2)}) copy-start(bf16[1,512,2048]{2,1,0:T(8,128)(2,1)} %param.37) | copy-start | bytes 6291460
  6.5 20.8 %copy-start.7 = (s32[128,2]{0,1:T(2,128)S(1)}, s32[128,2]{0,1:T(2,128)}, u32[]{:S(2)}) copy-start(s32[128,2]{0,1:T(2,128)} %param.38) | copy-start | bytes 3076
  6.5 22.3 %copy-start.4 = (bf16[256,512]{1,0:T(8,128)(2,1)S(1)}, bf16[256,512]{1,0:T(8,128)(2,1)}, u32[]{:S(2)}) copy-start(bf16[256,512]{1,0:T(8,128)(2,1)} %param.23) | copy-start | bytes 786436
  6.5 88.9 %all-gather.4.cloned.1.call-start = ((), (), s32[]{:S(2)}) async-start(), calls=%async_computation.6 | async-start | bytes 2129920 | tf_op jit(solution)/shard_map/all_gather | solution.py:162
  7.3 315.2 %all-gather.6.cloned.1.call-start = ((), (), s32[]{:S(2)}) async-start(), calls=%async_computation.7 | async-start | bytes 4259840 | tf_op jit(solution)/shard_map/all_gather | solution.py:163
  8.3 20.6 %copy-start.12 = (f32[64]{0:T(128)S(1)}, f32[64]{0:T(128)}, u32[]{:S(2)}) copy-start(f32[64]{0:T(128)} %param.29) | copy-start | bytes 772
  14.7 42.0 %all-to-all-start = ((bf16[64,256,64]{1,2,0:T(8,128)(2,1)}), bf16[64,256,64]{1,2,0:T(8,128)(2,1)}, u32[]{:S(2)}, u32[]{:S(2)}) async-start(bf16[64,256,64]{1,2,0:T(8,128)(2,1)} %stack.34), calls=%async_computation | async-start | bytes 4194304 | tf_op jit(solution)/shard_map/all_to_all | solution.py:160
  26.5 302.2 %all-gather.8.cloned.1.call-start = ((), (), s32[]{:S(2)}) async-start(), calls=%async_computation.8 | async-start | bytes 4259840 | tf_op jit(solution)/shard_map/all_gather | solution.py:164
  34.6 6.8 %copy-start.5 = (s32[256]{0:T(256)}, s32[256]{0:T(256)S(1)}, u32[]{:S(2)}) copy-start(s32[256]{0:T(256)S(1)} %fusion.78) | copy-start | bytes 3076
  334.8 5.9 %copy-start.1 = (f32[2048,256,4]{1,0,2:T(8,128)S(1)}, f32[2048,256,4]{1,0,2:T(8,128)}, u32[]{:S(2)}) copy-start(f32[2048,256,4]{1,0,2:T(8,128)} %get-tuple-element.357) | copy-start | bytes 25165828 | tf_op jit(solution)/shard_map/while
  347.7 5.9 %copy-start.1 = (f32[2048,256,4]{1,0,2:T(8,128)S(1)}, f32[2048,256,4]{1,0,2:T(8,128)}, u32[]{:S(2)}) copy-start(f32[2048,256,4]{1,0,2:T(8,128)} %get-tuple-element.357) | copy-start | bytes 25165828 | tf_op jit(solution)/shard_map/while
  360.5 5.9 %copy-start.1 = (f32[2048,256,4]{1,0,2:T(8,128)S(1)}, f32[2048,256,4]{1,0,2:T(8,128)}, u32[]{:S(2)}) copy-start(f32[2048,256,4]{1,0,2:T(8,128)} %get-tuple-element.357) | copy-start | bytes 25165828 | tf_op jit(solution)/shard_map/while
  373.4 5.9 %copy-start.1 = (f32[2048,256,4]{1,0,2:T(8,128)S(1)}, f32[2048,256,4]{1,0,2:T(8,128)}, u32[]{:S(2)}) copy-start(f32[2048,256,4]{1,0,2:T(8,128)} %get-tuple-element.357) | copy-start | bytes 25165828 | tf_op jit(solution)/shard_map/while
  386.3 5.9 %copy-start.1 = (f32[2048,256,4]{1,0,2:T(8,128)S(1)}, f32[2048,256,4]{1,0,2:T(8,128)}, u32[]{:S(2)}) copy-start(f32[2048,256,4]{1,0,2:T(8,128)} %get-tuple-element.357) | copy-start | bytes 25165828 | tf_op jit(solution)/shard_map/while
  399.1 5.9 %copy-start.1 = (f32[2048,256,4]{1,0,2:T(8,128)S(1)}, f32[2048,256,4]{1,0,2:T(8,128)}, u32[]{:S(2)}) copy-start(f32[2048,256,4]{1,0,2:T(8,128)} %get-tuple-element.357) | copy-start | bytes 25165828 | tf_op jit(solution)/shard_map/while
  412.0 5.9 %copy-start.1 = (f32[2048,256,4]{1,0,2:T(8,128)S(1)}, f32[2048,256,4]{1,0,2:T(8,128)}, u32[]{:S(2)}) copy-start(f32[2048,256,4]{1,0,2:T(8,128)} %get-tuple-element.357) | copy-start | bytes 25165828 | tf_op jit(solution)/shard_map/while
  424.9 5.9 %copy-start.1 = (f32[2048,256,4]{1,0,2:T(8,128)S(1)}, f32[2048,256,4]{1,0,2:T(8,128)}, u32[]{:S(2)}) copy-start(f32[2048,256,4]{1,0,2:T(8,128)} %get-tuple-element.357) | copy-start | bytes 25165828 | tf_op jit(solution)/shard_map/while
  436.0 4.9 copy-start.3
  436.1 5.2 copy-start.9
  480.9 9.4 %copy-start.13 = (bf16[1,2048,512]{2,1,0:T(8,128)(2,1)S(1)}, bf16[1,2048,512]{2,1,0:T(8,128)(2,1)}, u32[]{:S(2)}) copy-start(bf16[1,2048,512]{2,1,0:T(8,128)(2,1)} %param.36) | copy-start | bytes 6291460
  488.3 2.0 copy-start.2
  515.9 11.3 %copy-start.8 = (s32[128,2]{0,1:T(2,128)S(1)}, s32[128,2]{0,1:T(2,128)}, u32[]{:S(2)}) copy-start(s32[128,2]{0,1:T(2,128)} %param.38) | copy-start | bytes 3076
  515.9 11.5 %copy-start.10 = (pred[128,2]{0,1:T(4,128)(4,1)S(1)}, pred[128,2]{0,1:T(4,128)(4,1)}, u32[]{:S(2)}) copy-start(pred[128,2]{0,1:T(4,128)(4,1)} %get-tuple-element.221) | copy-start | bytes 772
  515.9 11.7 %copy-start.11 = (f32[128,2]{0,1:T(2,128)S(1)}, f32[128,2]{0,1:T(2,128)}, u32[]{:S(2)}) copy-start(f32[128,2]{0,1:T(2,128)} %param.39) | copy-start | bytes 3076
  515.9 11.8 %copy-start.6 = (s32[256]{0:T(256)S(1)}, s32[256]{0:T(256)}, u32[]{:S(2)}) copy-start(s32[256]{0:T(256)} %copy-done.5) | copy-start | bytes 3076
  520.9 36.4 %all-to-all-start.5 = ((bf16[64,8,2048]{2,1,0:T(8,128)(2,1)}), bf16[64,8,2048]{2,1,0:T(8,128)(2,1)}, u32[]{:S(2)}, u32[]{:S(2)}) async-start(bf16[64,8,2048]{2,1,0:T(8,128)(2,1)} %reduce_sum.131), calls=%async_computation.5 | async-start | bytes 4194304 | tf_op jit(solution)/shard_map/all_to_all | solution.py:215
Sparse Core Ops, SparseCore 0:
  10.0 85.3 all-gather.3
  98.1 73.9 all-gather.5
  175.1 69.3 all-gather.7
